TPU v7x, 32 devices: a whole 2x2x4 slice. The times are simulated.
32 devices in a mesh: rep: 4 (over z), fs: 2 (over y), tp: 4 (over x, core).
Axes of the slice: x: 2, y: 2, z: 4, core: 2. Of those that a mesh axis runs over, the one named last changes fastest.
Arguments:
- inputs: bfloat16 [512, 4096], P('rep'), may hold values from -6 to 6
- cotangent: bfloat16 [512, 4096], P('rep'), may hold values from -6 to 6
- w_gate: bfloat16 [4096, 11264], P(None, ('fs', 'tp')), may hold values from -0.09375 to 0.09375
- w_upward: bfloat16 [4096, 11264], P(None, ('fs', 'tp')), may hold values from -0.09375 to 0.09375
- w_down: bfloat16 [11264, 4096], P(('fs', 'tp')), may hold values from -0.0546875 to 0.0546875
Outputs:
- grad_input: bfloat16 [512, 4096], P('rep')
- grad_gate: float32 [4096, 11264], P('rep', ('fs', 'tp'))
- grad_upward: float32 [4096, 11264], P('rep', ('fs', 'tp'))
- grad_down: float32 [11264, 4096], P(('fs', 'tp'), 'rep')
All inputs are finite; a program needn't handle non-finite values.
Results may differ from a plain program's by a relative error of at most 0.0049.
Values may be sent and summed in bfloat16 or wider, within the bound.
A program may use at most 128 MiB of HBM per device.

v0:
```python
import jax
import jax.numpy as jnp
from jax import lax
from jax.sharding import PartitionSpec as P


def contract_rows(left, right):
    return lax.dot_general(
        left, right, (((0,), (0,)), ((), ())), preferred_element_type=jnp.float32
    )


def contract_cols(left, right):
    return lax.dot_general(
        left, right, (((1,), (1,)), ((), ())), preferred_element_type=jnp.float32
    )


def local(inputs, cotangent, w_gate, w_upward, w_down):
    gate_pre = jnp.dot(inputs, w_gate, preferred_element_type=jnp.float32)
    up_pre = jnp.dot(inputs, w_upward, preferred_element_type=jnp.float32)
    sigmoid_gate = jax.nn.sigmoid(gate_pre)
    activated = gate_pre * sigmoid_gate
    hidden = (activated * up_pre).astype(jnp.bfloat16)
    hidden_grad = contract_cols(cotangent, w_down)
    gate_delta = (
        hidden_grad * up_pre * sigmoid_gate * (1.0 + gate_pre * (1.0 - sigmoid_gate))
    ).astype(jnp.bfloat16)
    up_delta = (hidden_grad * activated).astype(jnp.bfloat16)
    input_cols, cotangent_cols = (
        lax.all_to_all(inputs, "rep", split_axis=1, concat_axis=0, tiled=True),
        lax.all_to_all(cotangent, "rep", split_axis=1, concat_axis=0, tiled=True),
    )
    piece_gate = lax.all_gather(gate_delta, "rep", axis=0, tiled=True)
    piece_up = lax.all_gather(up_delta, "rep", axis=0, tiled=True)
    piece_hidden = lax.all_gather(hidden, "rep", axis=0, tiled=True)
    grad_gate = contract_rows(input_cols, piece_gate)
    grad_upward = contract_rows(input_cols, piece_up)
    grad_down = contract_rows(piece_hidden, cotangent_cols)
    input_terms = contract_cols(gate_delta, w_gate) + contract_cols(up_delta, w_upward)
    grad_input = lax.psum(input_terms, ("fs", "tp")).astype(jnp.bfloat16)
    return (grad_input, grad_gate, grad_upward, grad_down)


def solution(mesh):
    in_specs = (
        P("rep", None),
        P("rep", None),
        P(None, ("fs", "tp")),
        P(None, ("fs", "tp")),
        P(("fs", "tp"), None),
    )
    out_specs = (
        P("rep", None),
        P("rep", ("fs", "tp")),
        P("rep", ("fs", "tp")),
        P(("fs", "tp"), "rep"),
    )
    return jax.shard_map(local, mesh=mesh, in_specs=in_specs, out_specs=out_specs, check_vma=False)
```

profile of v0, /device:TPU:0, one launch (start us, length us, event | category | flops | bytes accessed | tf_op | source)
XLA Modules:
  0.0 190.2 jit_solution(5874101361756558968)
XLA Ops:
  7.2 0.0 copy-start.2
  7.2 0.0 all-gather.4.cloned.1.call-start
  7.2 0.0 copy-start
  7.2 8.6 %fusion.1 = f32[128,1408]{1,0:T(8,128)S(1)} fusion(bf16[128,4096]{1,0:T(8,128)(2,1)} %param.6, bf16[1408,4096]{1,0:T(8,128)(2,1)} %param.9), kind=kOutput, calls=%fused_computation.8 | convolution fusion | flops 1476395008 | bytes 13303808 | tf_op jit(solution)/shard_map/dot_general | solution.py:14
  15.8 0.0 copy-done.2
  15.8 0.0 copy-done
  15.8 0.0 copy-start.1
  15.8 1.8 fusion.2
  17.7 2.4 %copy-done.1 = bf16[4096,1408]{1,0:T(8,128)(2,1)S(1)} copy-done((bf16[4096,1408]{1,0:T(8,128)(2,1)S(1)}, bf16[4096,1408]{1,0:T(8,128)(2,1)}, u32[]{:S(2)}) %copy-start.1) | copy-done | bytes 11534360
  20.1 3.0 %multiply_convert_fusion = (bf16[128,1408]{1,0:T(8,128)(2,1)}, bf16[128,1408]{1,0:T(8,128)(2,1)}, bf16[128,1408]{1,0:T(8,128)(2,1)}) fusion(f32[128,1408]{1,0:T(8,128)S(1)} %fusion.2, f32[128,1408]{1,0:T(8,128)S(1)} %fusion.1, bf16[128,4096]{1,0:T(8,128)(2,1)S(1)} %copy-done.2, bf16[4096,1408]{1,0:T(8,128)(2,1)S(1)} %copy-done.1), kind=kOutput, calls=%fused_computation.3 | convolution fusion | flops 1479098368 | bytes 15106048 | tf_op jit(solution)/shard_map/dot_general | solution.py:21
  23.1 0.0 all-gather.4.cloned.1.call-update
  23.1 0.0 all-gather.6.cloned.1.call-start
  23.2 0.7 all-gather.6.cloned.1.call-update
  23.9 1.3 copy.13
  25.2 6.3 %all-to-all-start = ((bf16[128,4,1024]{0,2,1:T(8,128)(2,1)}), bf16[128,4,1024]{0,2,1:T(8,128)(2,1)S(1)}, u32[]{:S(2)}, u32[]{:S(2)}) async-start(bf16[128,4,1024]{0,2,1:T(8,128)(2,1)} %bitcast.27), calls=%async_computation | async-start | bytes 2097152 | tf_op jit(solution)/shard_map/all_to_all | solution.py:31
  31.5 0.7 all-gather.8.cloned.1.call-update
  32.3 0.0 copy-done.3
  32.3 1.3 copy.15
  33.6 9.5 %fusion.3 = f32[128,4096]{1,0:T(8,128)} fusion(bf16[128,1408]{1,0:T(8,128)(2,1)S(1)} %copy-done.4, bf16[4096,1408]{1,0:T(8,128)(2,1)} %param.7), kind=kOutput, calls=%fused_computation.10 | convolution fusion | flops 1476395008 | bytes 13991936 | tf_op jit(solution)/shard_map/dot_general | solution.py:14
  43.1 37.0 %all-to-all-done = bf16[128,4,1024]{0,2,1:T(8,128)(2,1)S(1)} async-done(((bf16[128,4,1024]{0,2,1:T(8,128)(2,1)}), bf16[128,4,1024]{0,2,1:T(8,128)(2,1)S(1)}, u32[]{:S(2)}, u32[]{:S(2)}) %all-to-all-start) | async-done | bytes 1048608 | tf_op jit(solution)/shard_map/all_to_all | solution.py:31
  80.1 4.3 %all-to-all-start.1 = ((bf16[128,4,1024]{0,2,1:T(8,128)(2,1)}), bf16[128,4,1024]{0,2,1:T(8,128)(2,1)}, u32[]{:S(2)}, u32[]{:S(2)}) async-start(bf16[128,4,1024]{0,2,1:T(8,128)(2,1)} %bitcast.5), calls=%async_computation.1 | async-start | bytes 2097152 | tf_op jit(solution)/shard_map/all_to_all | solution.py:32
  84.3 9.0 %convolution_add_fusion = f32[128,4096]{1,0:T(8,128)S(1)} fusion(f32[128,4096]{1,0:T(8,128)} %fusion.3, bf16[128,1408]{1,0:T(8,128)(2,1)} %get-tuple-element.18, bf16[4096,1408]{1,0:T(8,128)(2,1)} %param.8), kind=kOutput, calls=%fused_computation | convolution fusion | flops 1476919296 | bytes 16089088 | tf_op jit(solution)/shard_map/dot_general | solution.py:14
  93.3 59.1 %all-reduce.1 = bf16[128,4096]{1,0:T(8,128)(2,1)} all-reduce(f32[128,4096]{1,0:T(8,128)S(1)} %convolution_add_fusion), channel_id=1, replica_groups=mesh['rep'=4,'fs'=2,'tp'=4] {'fs','tp'}, use_global_device_ids=true, to_apply=%region_0.0 | all-reduce | flops 524288 | bytes 3145728 | tf_op jit(solution)/shard_map/psum | solution.py:41
  152.4 0.5 copy.14
  153.0 0.0 all-to-all-done.1
  153.0 1.5 copy.16
  154.5 0.0 all-gather.4.cloned.1.call-done
  154.5 5.6 %convolution_bitcast_fusion.1 = f32[1024,1408]{0,1:T(8,128)} fusion(bf16[512,1408]{1,0:T(8,128)(2,1)} %all-gather.4.cloned.1.call-done, bf16[512,1024]{1,0:T(8,128)(2,1)S(1)} %bitcast.29), kind=kOutput, calls=%fused_computation.2 | convolution fusion | flops 1476395008 | bytes 8257536 | tf_op jit(solution)/shard_map/dot_general | solution.py:8
  160.1 6.2 %copy.17 = f32[1024,1408]{1,0:T(8,128)} copy(f32[1024,1408]{0,1:T(8,128)} %convolution_bitcast_fusion.1) | data formatting | bytes 11534336
  166.3 5.6 %convolution_bitcast_fusion = f32[1024,1408]{0,1:T(8,128)} fusion(bf16[512,1408]{1,0:T(8,128)(2,1)} %all-gather.6.cloned.1.call-done, bf16[512,1024]{1,0:T(8,128)(2,1)S(1)} %bitcast.30), kind=kOutput, calls=%fused_computation.1 | convolution fusion | flops 1476395008 | bytes 8257536 | tf_op jit(solution)/shard_map/dot_general | solution.py:8
  171.9 6.2 %copy.18 = f32[1024,1408]{1,0:T(8,128)} copy(f32[1024,1408]{0,1:T(8,128)} %convolution_bitcast_fusion) | data formatting | bytes 11534336
  178.1 5.6 %fusion.4 = f32[1408,1024]{1,0:T(8,128)} fusion(bf16[512,1408]{1,0:T(8,128)(2,1)} %all-gather.8.cloned.1.call-done, bf16[512,1024]{1,0:T(8,128)(2,1)S(1)} %bitcast.28), kind=kOutput, calls=%fused_computation.11 | convolution fusion | flops 1476395008 | bytes 8257536 | tf_op jit(solution)/shard_map/dot_general | solution.py:8
  (6 shorter events, 0.0 us)
Async XLA Ops:
  7.2 8.6 %copy-start.2 = (bf16[128,4096]{1,0:T(8,128)(2,1)S(1)}, bf16[128,4096]{1,0:T(8,128)(2,1)}, u32[]{:S(2)}) copy-start(bf16[128,4096]{1,0:T(8,128)(2,1)} %param.5) | copy-start | bytes 3145732
  7.2 147.3 %all-gather.4.cloned.1.call-start = ((), (), s32[]{:S(2)}) async-start(), calls=%async_computation.2 | async-start | bytes 1802240 | tf_op jit(solution)/shard_map/all_gather | solution.py:34
  7.2 8.6 %copy-start = (bf16[4096,1408]{1,0:T(8,128)(2,1)S(1)}, bf16[4096,1408]{1,0:T(8,128)(2,1)}, u32[]{:S(2)}) copy-start(bf16[4096,1408]{1,0:T(8,128)(2,1)} %param.7) | copy-start | bytes 34603012
  15.8 4.3 %copy-start.1 = (bf16[4096,1408]{1,0:T(8,128)(2,1)S(1)}, bf16[4096,1408]{1,0:T(8,128)(2,1)}, u32[]{:S(2)}) copy-start(bf16[4096,1408]{1,0:T(8,128)(2,1)} %param.8) | copy-start | bytes 34603012
  23.1 9.2 %copy-start.3 = (bf16[128,4096]{1,0:T(8,128)(2,1)S(1)}, bf16[128,4096]{1,0:T(8,128)(2,1)}, u32[]{:S(2)}) copy-start(bf16[128,4096]{1,0:T(8,128)(2,1)} %param.6) | copy-start | bytes 3145732
  23.1 10.5 %copy-start.4 = (bf16[128,1408]{1,0:T(8,128)(2,1)S(1)}, bf16[128,1408]{1,0:T(8,128)(2,1)}, u32[]{:S(2)}) copy-start(bf16[128,1408]{1,0:T(8,128)(2,1)} %get-tuple-element.17) | copy-start | bytes 1081348
  23.1 143.2 %all-gather.6.cloned.1.call-start = ((), (), s32[]{:S(2)}) async-start(), calls=%async_computation.3 | async-start | bytes 1802240 | tf_op jit(solution)/shard_map/all_gather | solution.py:35
  25.2 54.9 %all-to-all-start = ((bf16[128,4,1024]{0,2,1:T(8,128)(2,1)}), bf16[128,4,1024]{0,2,1:T(8,128)(2,1)S(1)}, u32[]{:S(2)}, u32[]{:S(2)}) async-start(bf16[128,4,1024]{0,2,1:T(8,128)(2,1)} %bitcast.27), calls=%async_computation | async-start | bytes 2097152 | tf_op jit(solution)/shard_map/all_to_all | solution.py:31
  31.5 146.6 %all-gather.8.cloned.1.call-start = ((), (), s32[]{:S(2)}) async-start(), calls=%async_computation.4 | async-start | bytes 1802240 | tf_op jit(solution)/shard_map/all_gather | solution.py:36
  80.1 72.9 %all-to-all-start.1 = ((bf16[128,4,1024]{0,2,1:T(8,128)(2,1)}), bf16[128,4,1024]{0,2,1:T(8,128)(2,1)}, u32[]{:S(2)}, u32[]{:S(2)}) async-start(bf16[128,4,1024]{0,2,1:T(8,128)(2,1)} %bitcast.5), calls=%async_computation.1 | async-start | bytes 2097152 | tf_op jit(solution)/shard_map/all_to_all | solution.py:32
Sparse Core Ops, SparseCore 0:
  23.2 57.4 all-gather.3
  82.3 48.3 all-gather.5
  132.3 33.8 all-gather.7
where the time goes:
time: 191 us; the launch traced here: 190 us
  blocking collectives  59.1 us (31%)
  matrix products  48.6 us (25%)
  waiting for transfers between devices  38.5 us (20%)
  local copies, waits for them, and re-layouts  19.5 us (10%)
  between operations  13.9 us (7%)
  starting transfers between devices  10.7 us (6%)
    psum x1, blocking collectives, local(): grad_input = lax.psum(input_terms, ('fs', 'tp')).astype(jnp.bfloat16)  59.1 us
    all_to_all x1, waiting for transfers between devices, local(): lax.all_to_all(inputs, 'rep', split_axis=1, concat_axis=0, tiled=True)  37 us
    dot_general x3, matrix products, contract_cols(): lax.dot_general(left, right, (((1,), (1,)), ((), ())), preferred_element_...  27 us
    unnamed x14, local copies, waits for them, and re-layouts  17.5 us
    dot_general x3, matrix products, contract_rows(): lax.dot_general(left, right, (((0,), (0,)), ((), ())), preferred_element_...  16.7 us
    all_to_all x1, starting transfers between devices, local(): lax.all_to_all(inputs, 'rep', split_axis=1, concat_axis=0, tiled=True)  6.35 us
    all_to_all x1, starting transfers between devices, local(): lax.all_to_all(cotangent, 'rep', split_axis=1, concat_axis=0, tiled=True)  4.27 us
  transfers between devices with their start and end apart: 5, of which 1 were waited for; matrix products, arithmetic and copies ran while one was open for 25% of the time, Pallas kernels for 0%

commit v1 on v0

--- a/solution.py
+++ b/solution.py
@@ -1,7 +1,15 @@
+import functools
 import jax
 import jax.numpy as jnp
 from jax import lax
 from jax.sharding import PartitionSpec as P
+
+
+def lift_numbers(xx, lane_axis):
+    return jnp.sum(lax.all_gather(xx, lane_axis), 0)
+
+
+unit_mark = functools.partial(lift_numbers, lane_axis=("fs", "tp"))
 
 
 def contract_rows(left, right):
@@ -38,7 +46,7 @@
     grad_upward = contract_rows(input_cols, piece_up)
     grad_down = contract_rows(piece_hidden, cotangent_cols)
     input_terms = contract_cols(gate_delta, w_gate) + contract_cols(up_delta, w_upward)
-    grad_input = lax.psum(input_terms, ("fs", "tp")).astype(jnp.bfloat16)
+    grad_input = unit_mark(input_terms).astype(jnp.bfloat16)
     return (grad_input, grad_gate, grad_upward, grad_down)
 
 

time: 191 us -> 265 us (1.39)
  waiting for transfers between devices: 38.5 us -> 165 us
  blocking collectives: 59.1 us -> 0 us
  other arithmetic: 0 us -> 8.43 us
    all_gather x0 -> x1, waiting for transfers between devices: none -> 84.9 us  [lift_numbers(): return jnp.sum(lax.all_gather(xx, lane_axis), 0)]
    psum x1 -> x0, blocking collectives: 59.1 us -> none  [local(): grad_input = lax.psum(input_terms, ('fs', 'tp')).astype(jnp.bfloat16)]
    all_to_all x1, waiting for transfers between devices: 0.01 us -> 35.6 us  [local(): lax.all_to_all(cotangent, 'rep', split_axis=1, concat_axis=0, tiled=True)]
    reduce_sum x0 -> x1, other arithmetic: none -> 8.43 us  [lift_numbers(): return jnp.sum(lax.all_gather(xx, lane_axis), 0)]
    all_gather x1, waiting for transfers between devices: 0.01 us -> 5.83 us  [local(): piece_hidden = lax.all_gather(hidden, 'rep', axis=0, tiled=True)]
  transfers between devices with their start and end apart: 5 -> 6, of which waited for: 1 -> 4; matrix products, arithmetic and copies ran while one was open for 25% -> 19% of each run, Pallas kernels for 0% -> 0%
where the time goes in v1:
time: 265 us; the launch traced here: 264 us
  waiting for transfers between devices  165 us (62%)
  matrix products  48 us (18%)
  local copies, waits for them, and re-layouts  18.6 us (7%)
  between operations  13.9 us (5%)
  starting transfers between devices  10 us (4%)
  other arithmetic  8.43 us (3%)
    all_gather x1, waiting for transfers between devices, lift_numbers(): return jnp.sum(lax.all_gather(xx, lane_axis), 0)  84.9 us
    all_to_all x1, waiting for transfers between devices, local(): lax.all_to_all(inputs, 'rep', split_axis=1, concat_axis=0, tiled=True)  37.5 us
    all_to_all x1, waiting for transfers between devices, local(): lax.all_to_all(cotangent, 'rep', split_axis=1, concat_axis=0, tiled=True)  35.6 us
    dot_general x3, matrix products, contract_cols(): lax.dot_general(left, right, (((1,), (1,)), ((), ())), preferred_element_...  26.4 us
    unnamed x14, local copies, waits for them, and re-layouts  17.5 us
    dot_general x3, matrix products, contract_rows(): lax.dot_general(left, right, (((0,), (0,)), ((), ())), preferred_element_...  16.8 us
    reduce_sum x1, other arithmetic, lift_numbers(): return jnp.sum(lax.all_gather(xx, lane_axis), 0)  8.43 us
    all_to_all x1, starting transfers between devices, local(): lax.all_to_all(inputs, 'rep', split_axis=1, concat_axis=0, tiled=True)  6.19 us
  transfers between devices with their start and end apart: 6, of which 4 were waited for; matrix products, arithmetic and copies ran while one was open for 19% of the time, Pallas kernels for 0%

profile of v1, /device:TPU:0, one launch (start us, length us, event | category | flops | bytes accessed | tf_op | source)
XLA Modules:
  0.0 264.2 jit_solution(18267900097118225035)
XLA Ops:
  7.2 0.0 all-gather.6.cloned.1.call-start
  7.2 0.0 copy-start
  7.2 8.6 %fusion.1 = f32[128,1408]{1,0:T(8,128)S(1)} fusion(bf16[128,4096]{1,0:T(8,128)(2,1)} %param.6, bf16[1408,4096]{1,0:T(8,128)(2,1)} %param.9), kind=kOutput, calls=%fused_computation.8 | convolution fusion | flops 1476395008 | bytes 13303808 | tf_op jit(solution)/shard_map/dot_general | solution.py:22
  15.8 1.8 fusion.2
  17.7 2.4 copy-done.1
  20.1 3.0 %multiply_convert_fusion = (bf16[128,1408]{1,0:T(8,128)(2,1)}, bf16[128,1408]{1,0:T(8,128)(2,1)}, bf16[128,1408]{1,0:T(8,128)(2,1)}) fusion(f32[128,1408]{1,0:T(8,128)S(1)} %fusion.2, f32[128,1408]{1,0:T(8,128)S(1)} %fusion.1, bf16[128,4096]{1,0:T(8,128)(2,1)S(1)} %copy-done.2, bf16[4096,1408]{1,0:T(8,128)(2,1)S(1)} %copy-done.1), kind=kOutput, calls=%fused_computation.3 | convolution fusion | flops 1479098368 | bytes 15106048 | tf_op jit(solution)/shard_map/dot_general | solution.py:29
  23.1 0.0 all-gather.6.cloned.1.call-update
  23.1 0.0 all-gather.8.cloned.1.call-start
  23.2 0.7 all-gather.8.cloned.1.call-update
  23.9 0.0 all-gather.10.cloned.1.call-start
  23.9 0.7 all-gather.10.cloned.1.call-update
  24.6 0.0 all-gather.12.cloned.1.call-start
  24.7 8.2 %fusion.3 = f32[128,4096]{1,0:T(8,128)S(1)} fusion(bf16[128,1408]{1,0:T(8,128)(2,1)} %get-tuple-element.17, bf16[4096,1408]{1,0:T(8,128)(2,1)} %param.7), kind=kOutput, calls=%fused_computation.10 | convolution fusion | flops 1476395008 | bytes 13991936 | tf_op jit(solution)/shard_map/dot_general | solution.py:22
  32.9 9.6 %convolution_add_fusion = f32[128,4096]{1,0:T(8,128)} fusion(f32[128,4096]{1,0:T(8,128)S(1)} %fusion.3, bf16[128,1408]{1,0:T(8,128)(2,1)S(1)} %copy-done.4, bf16[4096,1408]{1,0:T(8,128)(2,1)} %param.8), kind=kOutput, calls=%fused_computation | convolution fusion | flops 1476919296 | bytes 16089088 | tf_op jit(solution)/shard_map/dot_general | solution.py:22
  42.5 0.0 all-gather.12.cloned.1.call-update
  42.5 1.3 copy.13
  43.8 6.2 %all-to-all-start = ((bf16[128,4,1024]{0,2,1:T(8,128)(2,1)}), bf16[128,4,1024]{0,2,1:T(8,128)(2,1)S(1)}, u32[]{:S(2)}, u32[]{:S(2)}) async-start(bf16[128,4,1024]{0,2,1:T(8,128)(2,1)} %bitcast.1), calls=%async_computation | async-start | bytes 2097152 | tf_op jit(solution)/shard_map/all_to_all | solution.py:39
  50.0 1.3 copy.15
  51.3 37.5 %all-to-all-done = bf16[128,4,1024]{0,2,1:T(8,128)(2,1)S(1)} async-done(((bf16[128,4,1024]{0,2,1:T(8,128)(2,1)}), bf16[128,4,1024]{0,2,1:T(8,128)(2,1)S(1)}, u32[]{:S(2)}, u32[]{:S(2)}) %all-to-all-start) | async-done | bytes 1048608 | tf_op jit(solution)/shard_map/all_to_all | solution.py:39
  88.8 3.7 %all-to-all-start.1 = ((bf16[128,4,1024]{0,2,1:T(8,128)(2,1)}), bf16[128,4,1024]{0,2,1:T(8,128)(2,1)S(1)}, u32[]{:S(2)}, u32[]{:S(2)}) async-start(bf16[128,4,1024]{0,2,1:T(8,128)(2,1)} %bitcast.6), calls=%async_computation.1 | async-start | bytes 2097152 | tf_op jit(solution)/shard_map/all_to_all | solution.py:40
  92.5 0.5 copy.14
  93.1 35.6 %all-to-all-done.1 = bf16[128,4,1024]{0,2,1:T(8,128)(2,1)S(1)} async-done(((bf16[128,4,1024]{0,2,1:T(8,128)(2,1)}), bf16[128,4,1024]{0,2,1:T(8,128)(2,1)S(1)}, u32[]{:S(2)}, u32[]{:S(2)}) %all-to-all-start.1) | async-done | bytes 1048608 | tf_op jit(solution)/shard_map/all_to_all | solution.py:40
  128.7 0.5 copy.16
  129.2 0.0 all-gather.6.cloned.1.call-done
  129.3 5.6 %convolution_bitcast_fusion.1 = f32[1024,1408]{0,1:T(8,128)} fusion(bf16[512,1408]{1,0:T(8,128)(2,1)} %all-gather.6.cloned.1.call-done, bf16[512,1024]{1,0:T(8,128)(2,1)S(1)} %bitcast.31), kind=kOutput, calls=%fused_computation.2 | convolution fusion | flops 1476395008 | bytes 8257536 | tf_op jit(solution)/shard_map/dot_general | solution.py:16
  134.9 6.2 %copy.17 = f32[1024,1408]{1,0:T(8,128)} copy(f32[1024,1408]{0,1:T(8,128)} %convolution_bitcast_fusion.1) | data formatting | bytes 11534336
  141.1 5.6 %convolution_bitcast_fusion = f32[1024,1408]{0,1:T(8,128)} fusion(bf16[512,1408]{1,0:T(8,128)(2,1)} %all-gather.8.cloned.1.call-done, bf16[512,1024]{1,0:T(8,128)(2,1)S(1)} %bitcast.32), kind=kOutput, calls=%fused_computation.1 | convolution fusion | flops 1476395008 | bytes 8257536 | tf_op jit(solution)/shard_map/dot_general | solution.py:16
  146.7 6.2 %copy.18 = f32[1024,1408]{1,0:T(8,128)} copy(f32[1024,1408]{0,1:T(8,128)} %convolution_bitcast_fusion) | data formatting | bytes 11534336
  152.9 5.8 %all-gather.10.cloned.1.call-done = bf16[512,1408]{1,0:T(8,128)(2,1)} async-done(((bf16[128,1408]{1,0:T(8,128)(2,1)}), bf16[512,1408]{1,0:T(8,128)(2,1)}) %all-gather.10.cloned.1.call-update) | async-done | bytes 1441808 | tf_op jit(solution)/shard_map/all_gather | solution.py:44
  158.8 5.6 %fusion.4 = f32[1408,1024]{1,0:T(8,128)} fusion(bf16[512,1408]{1,0:T(8,128)(2,1)} %all-gather.10.cloned.1.call-done, bf16[512,1024]{1,0:T(8,128)(2,1)S(1)} %bitcast.30), kind=kOutput, calls=%fused_computation.11 | convolution fusion | flops 1476395008 | bytes 8257536 | tf_op jit(solution)/shard_map/dot_general | solution.py:16
  164.3 84.9 %all-gather.12.cloned.1.call-done = f32[1024,4096]{1,0:T(8,128)} async-done(((f32[128,4096]{1,0:T(8,128)}), f32[1024,4096]{1,0:T(8,128)}) %all-gather.12.cloned.1.call-update) | async-done | bytes 16777232 | tf_op jit(solution)/shard_map/all_gather | solution.py:9
  249.2 8.4 %reduce_sum.9 = bf16[128,4096]{1,0:T(8,128)(2,1)} reduce(f32[8,128,4096]{2,1,0:T(8,128)} %bitcast.27, f32[]{:T(128)} %constant.1.clone.1), dimensions={0}, to_apply=%region_0.0 | reduce | flops 3670016 | bytes 17825796 | tf_op jit(solution)/shard_map/reduce_sum | solution.py:9
  (9 shorter events, 0.0 us)
Async XLA Ops:
  7.2 8.6 %copy-start.2 = (bf16[128,4096]{1,0:T(8,128)(2,1)S(1)}, bf16[128,4096]{1,0:T(8,128)(2,1)}, u32[]{:S(2)}) copy-start(bf16[128,4096]{1,0:T(8,128)(2,1)} %param.5) | copy-start | bytes 3145732
  7.2 122.1 %all-gather.6.cloned.1.call-start = ((), (), s32[]{:S(2)}) async-start(), calls=%async_computation.2 | async-start | bytes 1802240 | tf_op jit(solution)/shard_map/all_gather | solution.py:42
  7.2 8.6 %copy-start = (bf16[4096,1408]{1,0:T(8,128)(2,1)S(1)}, bf16[4096,1408]{1,0:T(8,128)(2,1)}, u32[]{:S(2)}) copy-start(bf16[4096,1408]{1,0:T(8,128)(2,1)} %param.7) | copy-start | bytes 34603012
  15.8 4.3 %copy-start.1 = (bf16[4096,1408]{1,0:T(8,128)(2,1)S(1)}, bf16[4096,1408]{1,0:T(8,128)(2,1)}, u32[]{:S(2)}) copy-start(bf16[4096,1408]{1,0:T(8,128)(2,1)} %param.8) | copy-start | bytes 34603012
  23.1 118.0 %all-gather.8.cloned.1.call-start = ((), (), s32[]{:S(2)}) async-start(), calls=%async_computation.3 | async-start | bytes 1802240 | tf_op jit(solution)/shard_map/all_gather | solution.py:43
  23.9 134.9 %all-gather.10.cloned.1.call-start = ((), (), s32[]{:S(2)}) async-start(), calls=%async_computation.4 | async-start | bytes 1802240 | tf_op jit(solution)/shard_map/all_gather | solution.py:44
  24.6 8.3 %copy-start.4 = (bf16[128,1408]{1,0:T(8,128)(2,1)S(1)}, bf16[128,1408]{1,0:T(8,128)(2,1)}, u32[]{:S(2)}) copy-start(bf16[128,1408]{1,0:T(8,128)(2,1)} %get-tuple-element.18) | copy-start | bytes 1081348
  24.6 224.6 %all-gather.12.cloned.1.call-start = ((), (), s32[]{:S(2)}) async-start(), calls=%async_computation.5 | async-start | bytes 18874368 | tf_op jit(solution)/shard_map/all_gather | solution.py:9
  42.5 7.5 %copy-start.3 = (bf16[128,4096]{1,0:T(8,128)(2,1)S(1)}, bf16[128,4096]{1,0:T(8,128)(2,1)}, u32[]{:S(2)}) copy-start(bf16[128,4096]{1,0:T(8,128)(2,1)} %param.6) | copy-start | bytes 3145732
  43.8 45.0 %all-to-all-start = ((bf16[128,4,1024]{0,2,1:T(8,128)(2,1)}), bf16[128,4,1024]{0,2,1:T(8,128)(2,1)S(1)}, u32[]{:S(2)}, u32[]{:S(2)}) async-start(bf16[128,4,1024]{0,2,1:T(8,128)(2,1)} %bitcast.1), calls=%async_computation | async-start | bytes 2097152 | tf_op jit(solution)/shard_map/all_to_all | solution.py:39
  88.8 39.9 %all-to-all-start.1 = ((bf16[128,4,1024]{0,2,1:T(8,128)(2,1)}), bf16[128,4,1024]{0,2,1:T(8,128)(2,1)S(1)}, u32[]{:S(2)}, u32[]{:S(2)}) async-start(bf16[128,4,1024]{0,2,1:T(8,128)(2,1)} %bitcast.6), calls=%async_computation.1 | async-start | bytes 2097152 | tf_op jit(solution)/shard_map/all_to_all | solution.py:40
Sparse Core Ops, SparseCore 0:
  23.3 46.7 all-gather.5
  71.6 52.1 all-gather.7
  125.4 33.3 all-gather.9
  160.5 88.7 all-gather.11
